TPU v7x, 32 devices: a whole 2x2x4 slice. The times are simulated.
32 devices in a mesh: fs: 8 (over z, x), tp: 4 (over y, core).
Axes of the slice: x: 2, y: 2, z: 4, core: 2. Of those that a mesh axis runs over, the one named last changes fastest.
Arguments:
- saved_input: bfloat16 [2048, 4096], P('fs'), may hold values from -8 to 8
- query_cotangent: bfloat16 [2048, 2048], P('fs', 'tp'), may hold values from -6 to 6
- layer_cotangent: bfloat16 [2048, 4096], P('fs'), may hold values from -8 to 8
- mixed_heads: bfloat16 [2048, 2048], P('fs', 'tp'), may hold values from -6 to 6
- query_basis: bfloat16 [4096, 256], P('fs'), may hold values from -0.125 to 0.125
- output_basis: bfloat16 [4096, 256], P('fs'), may hold values from -0.125 to 0.125
- query_master: float32 [4096, 2048], P('fs', 'tp'), may hold values from -3 to 3
- output_master: float32 [4096, 2048], P('fs', 'tp'), may hold values from -3 to 3
- query_first: float32 [256, 2048], P('fs', 'tp'), may hold values from -6 to 6
- query_second: float32 [256, 2048], P('fs', 'tp'), may hold values from 0.25 to 4
- output_first: float32 [256, 2048], P('fs', 'tp'), may hold values from -6 to 6
- output_second: float32 [256, 2048], P('fs', 'tp'), may hold values from 0.25 to 4
Outputs:
- query_weight: float32 [4096, 2048], P('fs', 'tp')
- output_weight: float32 [4096, 2048], P('fs', 'tp')
- query_step: float32 [4096, 2048], P('fs', 'tp')
- output_step: float32 [4096, 2048], P('fs', 'tp')
- query_first_new: float32 [256, 2048], P('fs', 'tp')
- query_second_new: float32 [256, 2048], P('fs', 'tp')
- output_first_new: float32 [256, 2048], P('fs', 'tp')
- output_second_new: float32 [256, 2048], P('fs', 'tp')
- query_copy: bfloat16 [4096, 2048], P(None, 'tp')
- output_copy: bfloat16 [4096, 2048], P(None, 'tp')
All inputs are finite; a program needn't handle non-finite values.
Results may differ from a plain program's by a relative error of at most 0.0028.
Values may be sent and summed in bfloat16 or wider, within the bound.
A program may use at most 64 MiB of HBM per device.

v0:
```python
import jax
import jax.numpy as jnp
from jax import lax
from jax.sharding import PartitionSpec as P

QW = 2048
RANK = 256


beta_one = 0.8
beta_two = 0.9
rate = 0.1


def moment_update(low, factor, first, second):
    scaled = low * factor
    first_new = beta_one * first + (1.0 - beta_one) * scaled
    second_new = beta_two * second + (1.0 - beta_two) * scaled * scaled
    direction = (first_new / jnp.sqrt(second_new)).astype(jnp.bfloat16)
    return (first_new, second_new, direction)


def contract_tokens(left, right):
    return lax.dot_general(
        left,
        right,
        (((0,), (0,)), ((), ())),
        precision=lax.Precision.HIGHEST,
        preferred_element_type=jnp.float32,
    )


def per_device(
    saved_input,
    query_cotangent,
    layer_cotangent,
    mixed_heads,
    query_basis,
    output_basis,
    query_master,
    output_master,
    query_first,
    query_second,
    output_first,
    output_second,
):
    query_coords = jnp.dot(
        saved_input,
        lax.all_gather(query_basis, "fs", axis=0, tiled=True),
        preferred_element_type=jnp.float32,
    )
    output_coords = jnp.dot(
        layer_cotangent,
        lax.all_gather(output_basis, "fs", axis=0, tiled=True),
        preferred_element_type=jnp.float32,
    )
    query_part = contract_tokens(query_coords, query_cotangent.astype(jnp.float32))
    output_part = contract_tokens(output_coords, mixed_heads.astype(jnp.float32))
    query_low, output_low = (
        lax.psum_scatter(query_part, "fs", scatter_dimension=0, tiled=True),
        lax.psum_scatter(output_part, "fs", scatter_dimension=0, tiled=True),
    )
    local_squares = jnp.sum(query_low * query_low) + jnp.sum(output_low * output_low)
    total_squares = lax.psum(local_squares, ("fs", "tp"))
    factor = 1.0 / jnp.sqrt(1.0 + total_squares / (2.0 * RANK * QW))
    qf, qs, qdir = moment_update(query_low, factor, query_first, query_second)
    of, osec, odir = moment_update(output_low, factor, output_first, output_second)
    query_whole, output_whole = (
        lax.all_gather(qdir, "fs", axis=0, tiled=True),
        lax.all_gather(odir, "fs", axis=0, tiled=True),
    )
    query_step = jnp.dot(query_basis, query_whole, preferred_element_type=jnp.float32)
    output_step = jnp.dot(output_basis, output_whole, preferred_element_type=jnp.float32)
    query_weight = query_master - rate * query_step
    output_weight = output_master - rate * output_step
    query_copy, output_copy = (
        lax.all_gather(query_weight.astype(jnp.bfloat16), "fs", axis=0, tiled=True),
        lax.all_gather(output_weight.astype(jnp.bfloat16), "fs", axis=0, tiled=True),
    )
    return (
        query_weight,
        output_weight,
        query_step,
        output_step,
        qf,
        qs,
        of,
        osec,
        query_copy,
        output_copy,
    )


def solution(mesh):
    placed = (
        P("fs", None),
        P("fs", "tp"),
        P("fs", None),
        P("fs", "tp"),
        P("fs", None),
        P("fs", None),
        P("fs", "tp"),
        P("fs", "tp"),
        P("fs", "tp"),
        P("fs", "tp"),
        P("fs", "tp"),
        P("fs", "tp"),
    )
    return jax.shard_map(
        per_device,
        mesh=mesh,
        in_specs=placed,
        out_specs=(
            P("fs", "tp"),
            P("fs", "tp"),
            P("fs", "tp"),
            P("fs", "tp"),
            P("fs", "tp"),
            P("fs", "tp"),
            P("fs", "tp"),
            P("fs", "tp"),
            P(None, "tp"),
            P(None, "tp"),
        ),
        check_vma=False,
    )
```

profile of v0, /device:TPU:0, one launch (start us, length us, event | category | flops | bytes accessed | tf_op | source)
XLA Modules:
  0.0 486.5 jit_solution(8330795833223261178)
XLA Ops:
  7.2 0.0 copy-start
  7.2 0.0 all-gather.7.cloned.1.call-start
  7.2 0.7 all-gather.7.cloned.1.call-update
  7.9 0.0 all-gather.5.cloned.1.call-start
  8.0 0.7 all-gather.5.cloned.1.call-update
  8.7 0.0 copy-start.7
  8.7 0.0 reduce-scatter.5.cloned.1.call-start
  8.7 53.2 %all-gather.7.cloned.1.call-done = bf16[4096,256]{1,0:T(8,128)(2,1)} async-done(((bf16[512,256]{1,0:T(8,128)(2,1)}), bf16[4096,256]{1,0:T(8,128)(2,1)}) %all-gather.7.cloned.1.call-update) | async-done | bytes 2097168 | tf_op jit(solution)/shard_map/all_gather | solution.py:54
  62.0 0.0 copy-done
  62.0 2.3 fusion.8
  64.3 0.0 copy-done.7
  64.3 1.2 fusion.9
  65.5 0.0 reduce-scatter.5.cloned.1.call-update
  65.5 0.0 copy-start.4
  65.5 0.0 reduce-scatter.3.cloned.1.call-start
  65.6 46.2 %all-gather.5.cloned.1.call-done = bf16[4096,256]{1,0:T(8,128)(2,1)} async-done(((bf16[512,256]{1,0:T(8,128)(2,1)}), bf16[4096,256]{1,0:T(8,128)(2,1)}) %all-gather.5.cloned.1.call-update) | async-done | bytes 2097168 | tf_op jit(solution)/shard_map/all_gather | solution.py:49
  111.7 2.9 fusion.6
  114.7 0.0 copy-start.8
  114.7 0.0 copy-start.2
  114.7 2.2 fusion.7
  116.9 0.0 reduce-scatter.3.cloned.1.call-update
  116.9 0.0 all-gather.11.cloned.1.call-start
  117.0 59.9 %reduce-scatter.5.cloned.1.call-done = f32[32,512]{1,0:T(8,128)} async-done(((f32[256,512]{1,0:T(8,128)}), f32[32,512]{1,0:T(8,128)}) %reduce-scatter.5.cloned.1.call-update) | async-done | bytes 65552 | tf_op jit(solution)/shard_map/reduce_scatter | solution.py:61
  176.9 1.5 multiply_reduce_fusion
  178.4 63.9 %reduce-scatter.3.cloned.1.call-done = f32[32,512]{1,0:T(8,128)} async-done(((f32[256,512]{1,0:T(8,128)}), f32[32,512]{1,0:T(8,128)}) %reduce-scatter.3.cloned.1.call-update) | async-done | bytes 65552 | tf_op jit(solution)/shard_map/reduce_scatter | solution.py:60
  242.3 1.5 multiply_reduce_fusion.1
  245.1 0.0 copy-done.4
  245.1 1.3 copy.23
  246.4 39.9 %psum.7 = f32[]{:T(128)} all-reduce(f32[]{:T(128)S(6)} %add.24), channel_id=1, replica_groups=mesh['fs'=8,'tp'=4] {'fs','tp'}, use_global_device_ids=true, to_apply=%region_4.0 | all-reduce | flops 1 | bytes 8 | tf_op jit(solution)/shard_map/psum | solution.py:64
  287.0 1.5 multiply_convert_fusion
  288.5 30.7 %all_gather.21 = bf16[256,512]{1,0:T(8,128)(2,1)S(1)} all-gather(bf16[32,512]{1,0:T(8,128)(2,1)S(1)} %get-tuple-element.24), channel_id=1, replica_groups=mesh['fs'=8,'tp'=4] {'fs'}, dimensions={0}, use_global_device_ids=true | all-gather | bytes 294912 | tf_op jit(solution)/shard_map/all_gather | solution.py:70
  319.3 0.0 copy-done.2
  319.3 2.8 fusion.2
  322.1 0.0 all-gather.11.cloned.1.call-update
  322.1 0.0 all-gather.9.cloned.1.call-start
  322.1 2.6 copy.22
  324.7 1.5 multiply_convert_fusion.1
  326.3 32.0 %all_gather.20 = bf16[256,512]{1,0:T(8,128)(2,1)S(1)} all-gather(bf16[32,512]{1,0:T(8,128)(2,1)S(1)} %get-tuple-element.27), channel_id=1, replica_groups=mesh['fs'=8,'tp'=4] {'fs'}, dimensions={0}, use_global_device_ids=true | all-gather | bytes 294912 | tf_op jit(solution)/shard_map/all_gather | solution.py:69
  358.3 3.1 fusion.3
  361.4 0.0 all-gather.9.cloned.1.call-update
  361.4 2.6 copy.25
  364.0 1.3 copy.27
  365.3 2.6 copy.24
  367.9 1.3 copy.26
  369.2 28.7 %all-gather.11.cloned.1.call-done = bf16[4096,512]{0,1:T(8,128)(2,1)} async-done(((bf16[512,512]{0,1:T(8,128)(2,1)}), bf16[4096,512]{0,1:T(8,128)(2,1)}) %all-gather.11.cloned.1.call-update) | async-done | bytes 4194320 | tf_op jit(solution)/shard_map/all_gather | solution.py:78
  397.9 6.4 %copy.29 = bf16[4096,512]{1,0:T(8,128)(2,1)} copy(bf16[4096,512]{0,1:T(8,128)(2,1)} %all-gather.11.cloned.1.call-done) | data formatting | bytes 8388608
  404.3 68.9 %all-gather.9.cloned.1.call-done = bf16[4096,512]{0,1:T(8,128)(2,1)} async-done(((bf16[512,512]{0,1:T(8,128)(2,1)}), bf16[4096,512]{0,1:T(8,128)(2,1)}) %all-gather.9.cloned.1.call-update) | async-done | bytes 4194320 | tf_op jit(solution)/shard_map/all_gather | solution.py:77
  473.2 6.4 %copy.28 = bf16[4096,512]{1,0:T(8,128)(2,1)} copy(bf16[4096,512]{0,1:T(8,128)(2,1)} %all-gather.9.cloned.1.call-done) | data formatting | bytes 8388608
  (11 shorter events, 0.0 us)
Async XLA Ops:
  7.2 54.8 %copy-start = (bf16[256,4096]{1,0:T(8,128)(2,1)S(1)}, bf16[256,4096]{1,0:T(8,128)(2,1)}, u32[]{:S(2)}) copy-start(bf16[256,4096]{1,0:T(8,128)(2,1)} %param.14) | copy-start | bytes 6291460
  7.2 54.8 %all-gather.7.cloned.1.call-start = ((), (), s32[]{:S(2)}) async-start(), calls=%async_computation.4 | async-start | bytes 2359296 | tf_op jit(solution)/shard_map/all_gather | solution.py:54
  7.9 103.8 %all-gather.5.cloned.1.call-start = ((), (), s32[]{:S(2)}) async-start(), calls=%async_computation.2 | async-start | bytes 2359296 | tf_op jit(solution)/shard_map/all_gather | solution.py:49
  8.7 55.6 %copy-start.7 = (bf16[256,512]{1,0:T(8,128)(2,1)S(1)}, bf16[256,512]{1,0:T(8,128)(2,1)}, u32[]{:S(2)}) copy-start(bf16[256,512]{1,0:T(8,128)(2,1)} %param.15) | copy-start | bytes 786436
  8.7 168.2 %reduce-scatter.5.cloned.1.call-start = ((), (), s32[]{:S(2)}) async-start(), calls=%async_computation.5 | async-start | bytes 589824 | tf_op jit(solution)/shard_map/reduce_scatter | solution.py:61
  65.5 179.5 %copy-start.4 = (f32[512,512]{1,0:T(8,128)S(1)}, f32[512,512]{1,0:T(8,128)}, u32[]{:S(2)}) copy-start(f32[512,512]{1,0:T(8,128)} %param.19) | copy-start | bytes 3145732
  65.5 176.8 %reduce-scatter.3.cloned.1.call-start = ((), (), s32[]{:S(2)}) async-start(), calls=%async_computation.3 | async-start | bytes 589824 | tf_op jit(solution)/shard_map/reduce_scatter | solution.py:60
  114.7 172.3 %copy-start.8 = (f32[32,512]{1,0:T(8,128)S(1)}, f32[32,512]{1,0:T(8,128)}, u32[]{:S(2)}) copy-start(f32[32,512]{1,0:T(8,128)} %param.23) | copy-start | bytes 196612
  114.7 204.6 %copy-start.2 = (bf16[512,256]{1,0:T(8,128)(2,1)S(1)}, bf16[512,256]{1,0:T(8,128)(2,1)}, u32[]{:S(2)}) copy-start(bf16[512,256]{1,0:T(8,128)(2,1)} %param.17) | copy-start | bytes 786436
  116.9 281.0 %all-gather.11.cloned.1.call-start = ((), (), s32[]{:S(2)}) async-start(), calls=%async_computation.7 | async-start | bytes 4718592 | tf_op jit(solution)/shard_map/all_gather | solution.py:78
  176.8 110.2 %copy-start.6 = (f32[32,512]{1,0:T(8,128)S(1)}, f32[32,512]{1,0:T(8,128)}, u32[]{:S(2)}) copy-start(f32[32,512]{1,0:T(8,128)} %reduce-scatter.5.cloned.1.call-done) | copy-start | bytes 196612
  322.1 2.7 copy-start.5
  322.1 2.7 copy-start.9
  322.1 36.2 %copy-start.3 = (bf16[512,256]{1,0:T(8,128)(2,1)S(1)}, bf16[512,256]{1,0:T(8,128)(2,1)}, u32[]{:S(2)}) copy-start(bf16[512,256]{1,0:T(8,128)(2,1)} %param.16) | copy-start | bytes 786436
  322.1 151.1 %all-gather.9.cloned.1.call-start = ((), (), s32[]{:S(2)}) async-start(), calls=%async_computation.6 | async-start | bytes 4718592 | tf_op jit(solution)/shard_map/all_gather | solution.py:77
  365.3 2.6 copy-start.1
Sparse Core Ops, SparseCore 0:
  10.1 51.7 all-gather.6
  64.1 47.6 all-gather.4
  115.7 61.1 reduce-scatter.4
  180.6 61.6 reduce-scatter.2
  322.2 75.6 all-gather.10
  400.4 72.8 all-gather.8
where the time goes:
time: 487 us; the launch traced here: 486 us
  waiting for transfers between devices  322 us (66%)
  blocking collectives  103 us (21%)
  local copies, waits for them, and re-layouts  24.5 us (5%)
  between operations  16.2 us (3%)
  matrix products  14.6 us (3%)
  other arithmetic  6.02 us (1%)
    all_gather x1, waiting for transfers between devices, per_device(): lax.all_gather(query_weight.astype(jnp.bfloat16), 'fs', axis=0, tiled=True)  68.9 us
    reduce_scatter x1, waiting for transfers between devices, per_device(): lax.psum_scatter(query_part, 'fs', scatter_dimension=0, tiled=True)  63.9 us
    reduce_scatter x1, waiting for transfers between devices, per_device(): lax.psum_scatter(output_part, 'fs', scatter_dimension=0, tiled=True)  59.9 us
    all_gather x1, waiting for transfers between devices, per_device(): lax.all_gather(output_basis, 'fs', axis=0, tiled=True)  53.2 us
    all_gather x1, waiting for transfers between devices, per_device(): lax.all_gather(query_basis, 'fs', axis=0, tiled=True)  46.2 us
    psum x1, blocking collectives, per_device(): total_squares = lax.psum(local_squares, ('fs', 'tp'))  39.9 us
    all_gather x1, blocking collectives, per_device(): lax.all_gather(qdir, 'fs', axis=0, tiled=True)  32 us
    all_gather x1, blocking collectives, per_device(): lax.all_gather(odir, 'fs', axis=0, tiled=True)  30.7 us
  transfers between devices with their start and end apart: 6, of which 6 were waited for; matrix products, arithmetic and copies ran while one was open for 6% of the time, Pallas kernels for 0%

commit v1 on v0

--- a/solution.py
+++ b/solution.py
@@ -1,6 +1,10 @@
+import functools
+
 import jax
 import jax.numpy as jnp
 from jax import lax
+from jax.experimental import pallas as pl
+from jax.experimental.pallas import tpu as pltpu
 from jax.sharding import PartitionSpec as P
 
 QW = 2048
@@ -90,6 +94,275 @@
         output_copy,
     )
 
+MESH = pl.DeviceIdType.MESH
+CHUNKS = 4
+
+
+def ring_kernel(n, m, *refs):
+    x_hbm, cot_hbm, basis, master_hbm, first, second = (
+        (refs[0], refs[2]),
+        (refs[1], refs[3]),
+        (refs[4], refs[5]),
+        (refs[6], refs[7]),
+        (refs[8], refs[10]),
+        (refs[9], refs[11]),
+    )
+    w_out, step_out, first_out, second_out, copy_out = (
+        (refs[12], refs[13]),
+        (refs[14], refs[15]),
+        (refs[16], refs[18]),
+        (refs[17], refs[19]),
+        (refs[20], refs[21]),
+    )
+    (
+        x_v, cot_v, master_v, mine_v, rows_v, coord_v, part_v, got_v, square_v, direction_v, w_v, step_v, gather_v,
+        in_sem, out_sem, local_sem, rows_sem, coord_sem, part_sem, square_sem, direction_sem, gather_sem,
+    ) = refs[22:]
+    f, t = lax.axis_index("fs"), lax.axis_index("tp")
+    me = f * m + t
+    rank_part = mine_v.shape[1]
+    block = basis[0].shape[0]
+    low_rows = first[0].shape[0]
+    rank = basis[0].shape[1]
+
+    loads = {}
+    for k in range(2):
+        loads["x", k] = pltpu.make_async_copy(x_hbm[k], x_v.at[k], in_sem.at[k])
+        loads["cot", k] = pltpu.make_async_copy(cot_hbm[k], cot_v.at[k], in_sem.at[2 + k])
+        loads["master", k] = pltpu.make_async_copy(master_hbm[k], master_v.at[k], in_sem.at[4 + k])
+    for copy in loads.values():
+        copy.start()
+
+    barrier = pltpu.get_barrier_semaphore()
+    for d in range(1, n * m):
+        other = lax.rem(me + d, n * m)
+        pl.semaphore_signal(barrier, inc=1, device_id={"fs": other // m, "tp": lax.rem(other, m)}, device_id_type=MESH)
+
+    chosen = lax.broadcasted_iota(jnp.int32, (rank_part, rank), 1) == (
+        lax.broadcasted_iota(jnp.int32, (rank_part, rank), 0) + t * rank_part
+    )
+    select = jnp.where(chosen, 1.0, 0.0).astype(jnp.bfloat16)
+    for k in range(2):
+        mine_v[k] = lax.dot_general(
+            select, basis[k][...], (((1,), (1,)), ((), ())), preferred_element_type=jnp.float32
+        ).astype(jnp.bfloat16)
+    pl.semaphore_wait(barrier, n * m - 1)
+
+    def remote(source, target, sems, index, device):
+        return pltpu.make_async_remote_copy(
+            src_ref=source,
+            dst_ref=target,
+            send_sem=sems.at[(0,) + index],
+            recv_sem=sems.at[(1,) + index],
+            device_id=device,
+            device_id_type=MESH,
+        )
+
+    sent = []
+    rows = {}
+    for k in range(2):
+        for d in range(1, n):
+            rows[k, d] = remote(mine_v.at[k], rows_v.at[k, d], rows_sem, (k, d), {"fs": lax.rem(f + d, n)})
+            rows[k, d].start()
+            sent.append(rows[k, d])
+
+    parts = {}
+    for k in range(2):
+        loads["x", k].wait()
+        total = jnp.zeros((rank_part, x_v.shape[1]), jnp.float32)
+        for d in range(n):
+            if d > 0:
+                rows[k, d].wait_recv()
+            source = lax.rem(f - d + n, n)
+            left = mine_v[k] if d == 0 else rows_v[k, d]
+            right = x_v[k, :, pl.ds(pl.multiple_of(source * block, block), block)]
+            total = total + lax.dot_general(left, right, (((1,), (1,)), ((), ())), preferred_element_type=jnp.float32)
+        high = total.astype(jnp.bfloat16)
+        coord_v[k, t, 0] = high
+        coord_v[k, t, 1] = (total - high.astype(jnp.float32)).astype(jnp.bfloat16)
+        coords = []
+        for d in range(1, m):
+            copy = remote(coord_v.at[k, t], coord_v.at[k, t], coord_sem, (k, d), {"tp": lax.rem(t + d, m)})
+            copy.start()
+            coords.append(copy)
+            sent.append(copy)
+        loads["cot", k].wait()
+        for copy in coords:
+            copy.wait_recv()
+        whole_high = coord_v[k, :, 0].reshape(rank, x_v.shape[1])
+        whole_low = coord_v[k, :, 1].reshape(rank, x_v.shape[1])
+        part = jnp.dot(whole_high, cot_v[k], preferred_element_type=jnp.float32) + jnp.dot(
+            whole_low, cot_v[k], preferred_element_type=jnp.float32
+        )
+        part_v[k] = part.reshape(n, low_rows, part.shape[1])
+        for d in range(1, n):
+            other = lax.rem(f + d, n)
+            parts[k, d] = remote(part_v.at[k, other], got_v.at[k, d], part_sem, (k, d), {"fs": other})
+            parts[k, d].start()
+            sent.append(parts[k, d])
+
+    lows = []
+    squares = jnp.zeros((), jnp.float32)
+    for k in range(2):
+        low = part_v[k, f]
+        for d in range(1, n):
+            parts[k, d].wait_recv()
+            low = low + got_v[k, d]
+        lows.append(low)
+        squares = squares + jnp.sum(low * low)
+    square_v[0] = jnp.full(square_v.shape[1:], squares, jnp.float32)
+    copies = []
+    for d in range(1, n * m):
+        other = lax.rem(me + d, n * m)
+        copy = remote(
+            square_v.at[0], square_v.at[d], square_sem, (d,), {"fs": other // m, "tp": lax.rem(other, m)}
+        )
+        copy.start()
+        copies.append(copy)
+        sent.append(copy)
+    for copy in copies:
+        copy.wait_recv()
+    total_squares = jnp.sum(square_v[...], axis=0)[:1, :1]
+    factor = 1.0 / jnp.sqrt(1.0 + total_squares / (2.0 * rank * (first[0].shape[1] * m)))
+
+    directions = []
+    for k in range(2):
+        new_first, new_second, direction = moment_update(lows[k], factor, first[k][...], second[k][...])
+        first_out[k][...] = new_first
+        second_out[k][...] = new_second
+        direction_v[k, f] = direction
+        for d in range(1, n):
+            copy = remote(
+                direction_v.at[k, f], direction_v.at[k, f], direction_sem, (k, d), {"fs": lax.rem(f + d, n)}
+            )
+            copy.start()
+            directions.append(copy)
+            sent.append(copy)
+
+    half = n // 2
+    z, x = f // 2, lax.rem(f, 2)
+    place = (1 - x) * z + x * (n - 1 - z)
+
+    def at(p):
+        p = lax.rem(p + 2 * n, n)
+        h = p // half
+        return (1 - h) * 2 * p + h * (2 * (n - 1 - p) + 1)
+
+    toward = (at(place + 1), at(place - 1))
+    origin = [[at(place - s), at(place + s)] for s in range(n)]
+    piece = block // CHUNKS
+    wholes = []
+    for k in range(2):
+        loads["master", k].wait()
+        for copy in directions[k * (n - 1) : (k + 1) * (n - 1)]:
+            copy.wait_recv()
+    local = []
+    ring = {}
+
+    def forward(s, k, c):
+        where = gather_v.at[k, origin[s][k], pl.ds(c * piece, piece)]
+        if s < n - 1:
+            ring[s, k, c] = remote(where, where, gather_sem, (k, s, c), {"fs": toward[k]})
+            ring[s, k, c].start()
+            sent.append(ring[s, k, c])
+        copy = pltpu.make_async_copy(
+            where,
+            copy_out[k].at[pl.ds(pl.multiple_of(origin[s][k] * block + c * piece, piece), piece)],
+            local_sem.at[k, s, c],
+        )
+        copy.start()
+        local.append(copy)
+
+    for c in range(CHUNKS):
+        for k in range(2):
+            span = pl.ds(c * piece, piece)
+            step = jnp.dot(
+                basis[k][span, :],
+                direction_v[k].reshape(rank, direction_v.shape[3]),
+                preferred_element_type=jnp.float32,
+            )
+            weight = master_v[k, span, :] - rate * step
+            gather_v[k, f, span] = weight.astype(jnp.bfloat16)
+            forward(0, k, c)
+            step_v[k, span] = step
+            w_v[k, span] = weight
+    for k in range(2):
+        for i, (source, target) in enumerate(((w_v, w_out), (step_v, step_out))):
+            copy = pltpu.make_async_copy(source.at[k], target[k], out_sem.at[i, k])
+            copy.start()
+            local.append(copy)
+    for s in range(1, n):
+        for c in range(CHUNKS):
+            for k in range(2):
+                ring[s - 1, k, c].wait_recv()
+                forward(s, k, c)
+    for copy in sent:
+        copy.wait_send()
+    for copy in local:
+        copy.wait()
+
+
+def fused_per_device(n, m, *args):
+    x, cot, _, _, basis = args[:5]
+    first = args[8]
+    block, rank = basis.shape
+    columns = cot.shape[1]
+    tokens, width = x.shape
+    part = rank // m
+    low_rows = first.shape[0]
+    big = jax.ShapeDtypeStruct((block, columns), jnp.float32)
+    small = jax.ShapeDtypeStruct(first.shape, jnp.float32)
+    copied = jax.ShapeDtypeStruct((width, columns), jnp.bfloat16)
+    hbm = pl.BlockSpec(memory_space=pl.ANY)
+    vmem = pl.BlockSpec(memory_space=pltpu.VMEM)
+    bf16, f32 = jnp.bfloat16, jnp.float32
+    dma = pltpu.SemaphoreType.DMA
+    return pl.pallas_call(
+        functools.partial(ring_kernel, n, m),
+        out_shape=(big,) * 4 + (small,) * 4 + (copied,) * 2,
+        in_specs=[hbm] * 4 + [vmem] * 2 + [hbm] * 2 + [vmem] * 4,
+        out_specs=(hbm,) * 4 + (vmem,) * 4 + (hbm,) * 2,
+        scratch_shapes=[
+            pltpu.VMEM((2, tokens, width), bf16),
+            pltpu.VMEM((2, tokens, columns), bf16),
+            pltpu.VMEM((2, block, columns), f32),
+            pltpu.VMEM((2, part, block), bf16),
+            pltpu.VMEM((2, n, part, block), bf16),
+            pltpu.VMEM((2, m, 2, part, tokens), bf16),
+            pltpu.VMEM((2, n, low_rows, columns), f32),
+            pltpu.VMEM((2, n, low_rows, columns), f32),
+            pltpu.VMEM((n * m, 8, 128), f32),
+            pltpu.VMEM((2, n, low_rows, columns), bf16),
+            pltpu.VMEM((2, block, columns), f32),
+            pltpu.VMEM((2, block, columns), f32),
+            pltpu.VMEM((2, n, block, columns), bf16),
+            dma((6,)),
+            dma((2, 2)),
+            dma((2, n, CHUNKS)),
+            dma((2, 2, n)),
+            dma((2, 2, m)),
+            dma((2, 2, n)),
+            dma((2, n * m)),
+            dma((2, 2, n)),
+            dma((2, 2, n - 1, CHUNKS)),
+        ],
+        compiler_params=pltpu.CompilerParams(
+            collective_id=0, has_side_effects=True, vmem_limit_bytes=50 * 2**20
+        ),
+    )(*args)
+
+
+def fits(n, m, *args):
+    basis, first = args[4], args[8]
+    return (
+        n % 2 == 0
+        and basis.shape[1] // n % 16 == 0
+        and basis.shape[1] // m % 16 == 0
+        and basis.shape[0] // n % (16 * CHUNKS) == 0
+        and basis.shape[0] // n % 128 == 0
+        and first.shape[1] // m % 128 == 0
+    )
+
 
 def solution(mesh):
     placed = (
@@ -106,21 +379,16 @@
         P("fs", "tp"),
         P("fs", "tp"),
     )
-    return jax.shard_map(
-        per_device,
-        mesh=mesh,
-        in_specs=placed,
-        out_specs=(
-            P("fs", "tp"),
-            P("fs", "tp"),
-            P("fs", "tp"),
-            P("fs", "tp"),
-            P("fs", "tp"),
-            P("fs", "tp"),
-            P("fs", "tp"),
-            P("fs", "tp"),
-            P(None, "tp"),
-            P(None, "tp"),
-        ),
-        check_vma=False,
-    )
+    n, m = mesh.shape["fs"], mesh.shape["tp"]
+
+    def step(*args):
+        body = functools.partial(fused_per_device, n, m) if fits(n, m, *args) else per_device
+        return jax.shard_map(
+            body,
+            mesh=mesh,
+            in_specs=placed,
+            out_specs=(P("fs", "tp"),) * 8 + (P(None, "tp"),) * 2,
+            check_vma=False,
+        )(*args)
+
+    return step

time: 487 us -> 179 us (0.37)
  waiting for transfers between devices: 322 us -> 0 us
  Pallas kernels: 0 us -> 159 us
  blocking collectives: 103 us -> 0 us
  between operations: 16.2 us -> 0.7 us
  matrix products: 14.6 us -> 0 us
  other arithmetic: 6.02 us -> 0 us
  local copies, waits for them, and re-layouts: 24.5 us -> 19.3 us
    all_gather x4 -> x0, waiting for transfers between devices: 197 us -> none  [the longest x1 68.9 us: per_device(): lax.all_gather(query_weight.astype(jnp.bfloat16), 'fs', axis=0, tiled=True)]
    pallas_call x0 -> x1, Pallas kernels: none -> 159 us  [fused_per_device(): pl.pallas_call(functools.partial(ring_kernel, n, m), out_shape=(big,) * 4...]
    reduce_scatter x2 -> x0, waiting for transfers between devices: 124 us -> none  [the longest x1 63.9 us: per_device(): lax.psum_scatter(query_part, 'fs', scatter_dimension=0, tiled=True)]
    all_gather x2 -> x0, blocking collectives: 62.8 us -> none  [the longest x1 32 us: per_device(): lax.all_gather(qdir, 'fs', axis=0, tiled=True)]
    psum x1 -> x0, blocking collectives: 39.9 us -> none  [per_device(): total_squares = lax.psum(local_squares, ('fs', 'tp'))]
    dot_general x6 -> x0, matrix products: 14.6 us -> none  [the longest x2 3.43 us: contract_tokens(): lax.dot_general(left, right, (((0,), (0,)), ((), ())), precision=lax.Prec...]
    unnamed x28 -> x34, local copies, waits for them, and re-layouts: 24.5 us -> 19.3 us
  transfers between devices with their start and end apart: 6 -> 0, of which waited for: 6 -> 0; matrix products, arithmetic and copies ran while one was open for 6% -> 0% of each run, Pallas kernels for 0% -> 0%
where the time goes in v1:
time: 179 us
  Pallas kernels  159 us (89%)
  local copies, waits for them, and re-layouts  19.3 us (11%)
    pallas_call x1, Pallas kernels, fused_per_device(): pl.pallas_call(functools.partial(ring_kernel, n, m), out_shape=(big,) * 4...  159 us
    unnamed x34, local copies, waits for them, and re-layouts  19.3 us

profile of v1, /device:TPU:0, one launch (start us, length us, event | category | flops | bytes accessed | tf_op | source)
XLA Modules:
  0.0 178.5 jit_solution(12289536332816453766)
XLA Ops:
  0.6 0.0 copy-start
  0.7 0.9 copy-done
  1.6 0.0 copy-start.1
  1.6 0.9 copy-done.1
  2.5 0.0 copy-start.2
  2.6 0.9 copy-done.2
  3.5 0.0 copy-start.3
  3.5 0.9 copy-done.3
  4.5 0.0 copy-start.4
  4.5 0.8 copy-done.4
  5.3 0.0 copy-start.5
  5.3 0.8 copy-done.5
  6.1 0.0 copy-start.6
  6.1 0.8 copy-done.6
  7.0 0.0 copy-start.7
  7.0 0.8 copy-done.7
  7.8 158.5 %shard_map.195 = (f32[512,512]{1,0:T(8,128)S(1)}, f32[512,512]{1,0:T(8,128)S(1)}, f32[512,512]{1,0:T(8,128)}, f32[512,512]{1,0:T(8,128)}, f32[32,512]{1,0:T(8,12...) custom-call(bf16[256,4096]{1,0:T(8,128)(2,1)} %refs_0_.1, ...), custom_call_target="tpu_custom_call" | custom-call | tf_op jit(solution)/shard_map/pallas_call | solution.py:320
  166.3 0.0 copy-start.11
  166.4 0.0 copy-start.10
  166.4 0.0 copy-start.9
  166.4 1.0 copy.32
  167.4 1.0 copy.33
  168.3 0.0 copy-done.11
  168.3 1.0 copy.34
  169.3 0.0 copy-done.10
  169.3 1.0 copy.35
  170.3 0.6 copy.36
  170.9 0.6 copy.37
  171.5 0.6 copy.38
  172.2 0.6 copy.39
  172.8 0.0 copy-done.9
  172.8 0.0 copy-start.8
  172.8 2.1 %copy.40 = bf16[4096,512]{1,0:T(8,128)(2,1)} copy(bf16[4096,512]{1,0:T(8,128)(2,1)S(1)} %copy-done.9) | data formatting | bytes 8388608
  174.9 1.6 copy-done.8
  176.5 2.0 %copy.41 = bf16[4096,512]{1,0:T(8,128)(2,1)} copy(bf16[4096,512]{1,0:T(8,128)(2,1)S(1)} %copy-done.8) | data formatting | bytes 8388608
Async XLA Ops:
  0.6 1.0 copy-start
  1.6 0.9 copy-start.1
  2.5 0.9 copy-start.2
  3.5 0.9 copy-start.3
  4.5 0.8 copy-start.4
  5.3 0.8 copy-start.5
  6.1 0.8 copy-start.6
  7.0 0.8 copy-start.7
  166.3 2.0 %copy-start.11 = (f32[512,512]{1,0:T(8,128)S(1)}, f32[512,512]{1,0:T(8,128)}, u32[]{:S(2)}) copy-start(f32[512,512]{1,0:T(8,128)} %get-tuple-element.22) | copy-start | bytes 3145732
  166.4 2.9 %copy-start.10 = (f32[512,512]{1,0:T(8,128)S(1)}, f32[512,512]{1,0:T(8,128)}, u32[]{:S(2)}) copy-start(f32[512,512]{1,0:T(8,128)} %get-tuple-element.23) | copy-start | bytes 3145732
  166.4 6.4 %copy-start.9 = (bf16[4096,512]{1,0:T(8,128)(2,1)S(1)}, bf16[4096,512]{1,0:T(8,128)(2,1)}, u32[]{:S(2)}) copy-start(bf16[4096,512]{1,0:T(8,128)(2,1)} %get-tuple-element.28) | copy-start | bytes 12582916
  172.8 3.7 %copy-start.8 = (bf16[4096,512]{1,0:T(8,128)(2,1)S(1)}, bf16[4096,512]{1,0:T(8,128)(2,1)}, u32[]{:S(2)}) copy-start(bf16[4096,512]{1,0:T(8,128)(2,1)} %get-tuple-element.29) | copy-start | bytes 12582916

commit v2 on v1

v2 whole, which is shorter than its diff:
```python
import functools

import jax
import jax.numpy as jnp
from jax import lax
from jax.experimental import pallas as pl
from jax.experimental.pallas import tpu as pltpu
from jax.sharding import PartitionSpec as P

QW = 2048
RANK = 256


beta_one = 0.8
beta_two = 0.9
rate = 0.1


def moment_update(low, factor, first, second):
    scaled = low * factor
    first_new = beta_one * first + (1.0 - beta_one) * scaled
    second_new = beta_two * second + (1.0 - beta_two) * scaled * scaled
    direction = (first_new / jnp.sqrt(second_new)).astype(jnp.bfloat16)
    return (first_new, second_new, direction)


def contract_tokens(left, right):
    return lax.dot_general(
        left,
        right,
        (((0,), (0,)), ((), ())),
        precision=lax.Precision.HIGHEST,
        preferred_element_type=jnp.float32,
    )


def per_device(
    saved_input,
    query_cotangent,
    layer_cotangent,
    mixed_heads,
    query_basis,
    output_basis,
    query_master,
    output_master,
    query_first,
    query_second,
    output_first,
    output_second,
):
    query_coords = jnp.dot(
        saved_input,
        lax.all_gather(query_basis, "fs", axis=0, tiled=True),
        preferred_element_type=jnp.float32,
    )
    output_coords = jnp.dot(
        layer_cotangent,
        lax.all_gather(output_basis, "fs", axis=0, tiled=True),
        preferred_element_type=jnp.float32,
    )
    query_part = contract_tokens(query_coords, query_cotangent.astype(jnp.float32))
    output_part = contract_tokens(output_coords, mixed_heads.astype(jnp.float32))
    query_low, output_low = (
        lax.psum_scatter(query_part, "fs", scatter_dimension=0, tiled=True),
        lax.psum_scatter(output_part, "fs", scatter_dimension=0, tiled=True),
    )
    local_squares = jnp.sum(query_low * query_low) + jnp.sum(output_low * output_low)
    total_squares = lax.psum(local_squares, ("fs", "tp"))
    factor = 1.0 / jnp.sqrt(1.0 + total_squares / (2.0 * RANK * QW))
    qf, qs, qdir = moment_update(query_low, factor, query_first, query_second)
    of, osec, odir = moment_update(output_low, factor, output_first, output_second)
    query_whole, output_whole = (
        lax.all_gather(qdir, "fs", axis=0, tiled=True),
        lax.all_gather(odir, "fs", axis=0, tiled=True),
    )
    query_step = jnp.dot(query_basis, query_whole, preferred_element_type=jnp.float32)
    output_step = jnp.dot(output_basis, output_whole, preferred_element_type=jnp.float32)
    query_weight = query_master - rate * query_step
    output_weight = output_master - rate * output_step
    query_copy, output_copy = (
        lax.all_gather(query_weight.astype(jnp.bfloat16), "fs", axis=0, tiled=True),
        lax.all_gather(output_weight.astype(jnp.bfloat16), "fs", axis=0, tiled=True),
    )
    return (
        query_weight,
        output_weight,
        query_step,
        output_step,
        qf,
        qs,
        of,
        osec,
        query_copy,
        output_copy,
    )

MESH = pl.DeviceIdType.MESH
CHUNKS = 4


def ring_kernel(n, m, *refs):
    x_hbm, cot_hbm, basis_hbm, master_hbm, first_hbm, second_hbm = (
        (refs[0], refs[2]),
        (refs[1], refs[3]),
        (refs[4], refs[5]),
        (refs[6], refs[7]),
        (refs[8], refs[10]),
        (refs[9], refs[11]),
    )
    w_out, step_out, first_out, second_out, gathered = (
        (refs[12], refs[13]),
        (refs[14], refs[15]),
        (refs[16], refs[18]),
        (refs[17], refs[19]),
        (refs[20], refs[21]),
    )
    (
        x_v, cot_v, basis, master_v, first, second,
        mine_v, rows_v, coord_v, part_v, pair_v, got_v, square_v, direction_v,
        in_sem, rows_sem, coord_sem, pair_sem, part_sem, square_sem, direction_sem, gather_sem,
    ) = refs[22:]
    f, t = lax.axis_index("fs"), lax.axis_index("tp")
    me = f * m + t
    rank_part, block = mine_v.shape[1:]
    rank = basis.shape[2]
    tokens = x_v.shape[1]
    columns = cot_v.shape[2]
    low_rows = first.shape[1]
    half = n // 2
    z, x = f // 2, lax.rem(f, 2)
    across = z * 2 + 1 - x

    def along(d, side=None):
        side = x if side is None else side
        return lax.rem(z + d + half, half) * 2 + side

    loads = {}
    for k in range(2):
        loads["basis", k] = pltpu.make_async_copy(basis_hbm[k], basis.at[k], in_sem.at[0, k])
    for i, (name, sources, target) in enumerate(
        (
            ("x", x_hbm, x_v),
            ("cot", cot_hbm, cot_v),
            ("first", first_hbm, first),
            ("second", second_hbm, second),
            ("master", master_hbm, master_v),
        )
    ):
        for k in range(2):
            loads[name, k] = pltpu.make_async_copy(sources[k], target.at[k], in_sem.at[1 + i, k])
    for copy in loads.values():
        copy.start()

    barrier = pltpu.get_barrier_semaphore()
    for d in range(1, n * m):
        other = lax.rem(me + d, n * m)
        pl.semaphore_signal(barrier, inc=1, device_id={"fs": other // m, "tp": lax.rem(other, m)}, device_id_type=MESH)

    chosen = lax.broadcasted_iota(jnp.int32, (rank_part, rank), 1) == (
        lax.broadcasted_iota(jnp.int32, (rank_part, rank), 0) + t * rank_part
    )
    select = jnp.where(chosen, 1.0, 0.0).astype(jnp.bfloat16)
    for k in range(2):
        loads["basis", k].wait()
        mine_v[k] = lax.dot_general(
            select, basis[k], (((1,), (1,)), ((), ())), preferred_element_type=jnp.float32
        ).astype(jnp.bfloat16)
    pl.semaphore_wait(barrier, n * m - 1)

    sent = []

    def send(source, target, sems, index, device):
        copy = pltpu.make_async_remote_copy(
            src_ref=source,
            dst_ref=target,
            send_sem=sems.at[(0,) + index],
            recv_sem=sems.at[(1,) + index],
            device_id=device,
            device_id_type=MESH,
        )
        copy.start()
        sent.append(copy)
        return copy

    def push(own, slots, sems, k):
        copies = {half: send(own, slots(half), sems, (k, half), {"fs": across})}
        for d in (1, half - 1, *range(2, half - 1)):
            copies[d] = send(own, slots(d), sems, (k, d), {"fs": along(d)})
        return copies

    def relay(copies, slots, sems, k):
        for d in (1, half - 1, *range(2, half - 1)):
            copies[d].wait_recv()
            copies[half + d] = send(slots(d), slots(half + d), sems, (k, half + d), {"fs": across})

    def rows_at(k):
        return lambda d: rows_v.at[k, d]

    rows = [push(mine_v.at[k], rows_at(k), rows_sem, k) for k in range(2)]

    def coordinates(k, d):
        source = along(-(d % half), x if d < half else 1 - x)
        left = mine_v[k] if d == 0 else rows_v[k, d]
        right = x_v[k, :, pl.ds(pl.multiple_of(source * block, block), block)]
        return lax.dot_general(left, right, (((1,), (1,)), ((), ())), preferred_element_type=jnp.float32)

    coords = []
    for k in range(2):
        if k == 0:
            relay(rows[0], rows_at(0), rows_sem, 0)
        loads["x", k].wait()
        total = coordinates(k, 0)
        for d in range(1, half):
            total = total + coordinates(k, d)
        if k == 0:
            relay(rows[1], rows_at(1), rows_sem, 1)
        for d in range(half, n):
            rows[k][d].wait_recv()
            total = total + coordinates(k, d)
        high = total.astype(jnp.bfloat16)
        coord_v[k, t, 0] = high
        coord_v[k, t, 1] = (total - high.astype(jnp.float32)).astype(jnp.bfloat16)
        coords.append(
            [
                send(coord_v.at[k, t], coord_v.at[k, t], coord_sem, (k, d), {"tp": lax.rem(t + d, m)})
                for d in range(1, m)
            ]
        )

    pairs = []
    for k in range(2):
        loads["cot", k].wait()
        for copy in coords[k]:
            copy.wait_recv()
        part = jnp.dot(
            coord_v[k, :, 0].reshape(rank, tokens), cot_v[k], preferred_element_type=jnp.float32
        ) + jnp.dot(coord_v[k, :, 1].reshape(rank, tokens), cot_v[k], preferred_element_type=jnp.float32)
        part_v[k] = part.reshape(n, low_rows, columns)
        pairs.append({})
        for d in (1, half - 1, *range(2, half - 1), 0):
            pairs[k][d] = send(
                part_v.at[k, along(d, 1 - x)], pair_v.at[k, d], pair_sem, (k, d), {"fs": across}
            )
    parts = []
    for k in range(2):
        parts.append({})
        for d in (1, half - 1, *range(2, half - 1)):
            pairs[k][d].wait_recv()
            pair_v[k, d] = pair_v[k, d] + part_v[k, along(d)]
            parts[k][d] = send(pair_v.at[k, d], got_v.at[k, d], part_sem, (k, d), {"fs": along(d)})

    lows = []
    squares = jnp.zeros((), jnp.float32)
    for k in range(2):
        pairs[k][0].wait_recv()
        low = pair_v[k, 0] + part_v[k, f]
        for d in range(1, half):
            parts[k][d].wait_recv()
            low = low + got_v[k, d]
        lows.append(low)
        squares = squares + jnp.sum(low * low)
    square_v[0] = jnp.full(square_v.shape[1:], squares, jnp.float32)
    copies = []
    for d in range(1, n * m):
        other = lax.rem(me + d, n * m)
        copies.append(
            send(square_v.at[0], square_v.at[d], square_sem, (d,), {"fs": other // m, "tp": lax.rem(other, m)})
        )
    for k in range(2):
        loads["first", k].wait()
        loads["second", k].wait()
    for copy in copies:
        copy.wait_recv()
    total_squares = jnp.sum(square_v[...], axis=0)[:1, :1]
    factor = 1.0 / jnp.sqrt(1.0 + total_squares / (2.0 * rank * (columns * m)))

    directions = []
    for k in range(2):
        new_first, new_second, direction = moment_update(lows[k], factor, first[k], second[k])
        direction_v[k, f] = direction
        own = direction_v.at[k, f]
        directions.append(push(own, lambda d: own, direction_sem, k))
        first_out[k][...] = new_first
        second_out[k][...] = new_second
    for k in range(2):
        for d in (1, half - 1, *range(2, half - 1)):
            directions[k][d].wait_recv()
            arrived = direction_v.at[k, along(-d)]
            directions[k][half + d] = send(arrived, arrived, direction_sem, (k, half + d), {"fs": across})

    place = (1 - x) * z + x * (n - 1 - z)

    def at(p):
        p = lax.rem(p + 2 * n, n)
        h = p // half
        return (1 - h) * 2 * p + h * (2 * (n - 1 - p) + 1)

    toward = (at(place + 1), at(place - 1))
    origin = [[at(place - s), at(place + s)] for s in range(n)]
    piece = block // CHUNKS
    for k in range(2):
        loads["master", k].wait()
        for d in range(half, n):
            directions[k][d].wait_recv()
    ring = {}

    def forward(s, k, c):
        where = gathered[k].at[pl.ds(pl.multiple_of(origin[s][k] * block + c * piece, piece), piece)]
        ring[s, k, c] = send(where, where, gather_sem, (k, s, c), {"fs": toward[k]})

    for c in range(CHUNKS):
        for k in range(2):
            span = pl.ds(c * piece, piece)
            step = jnp.dot(
                basis[k, span, :],
                direction_v[k].reshape(rank, columns),
                preferred_element_type=jnp.float32,
            )
            weight = master_v[k, span, :] - rate * step
            gathered[k][pl.ds(pl.multiple_of(f * block + c * piece, piece), piece)] = weight.astype(jnp.bfloat16)
            forward(0, k, c)
            step_out[k][span] = step
            w_out[k][span] = weight
    for s in range(1, n):
        for c in range(CHUNKS):
            for k in range(2):
                ring[s - 1, k, c].wait_recv()
                if s < n - 1:
                    forward(s, k, c)
    for copy in sent:
        copy.wait_send()


def write_kernel(count, *refs):
    sem = refs[2 * count]
    copies = [pltpu.make_async_copy(refs[i], refs[count + i], sem.at[i]) for i in range(count)]
    for copy in copies:
        copy.start()
    for copy in copies:
        copy.wait()


def fused_per_device(n, m, *args):
    x, cot, _, _, basis = args[:5]
    first = args[8]
    block, rank = basis.shape
    columns = cot.shape[1]
    tokens, width = x.shape
    part = rank // m
    low_rows = first.shape[0]
    bf16, f32 = jnp.bfloat16, jnp.float32
    kinds = [((block, columns), f32)] * 4 + [(first.shape, f32)] * 4 + [((width, columns), bf16)] * 2
    hbm = pl.BlockSpec(memory_space=pltpu.HBM)
    vmem = pl.BlockSpec(memory_space=pltpu.VMEM)
    dma = pltpu.SemaphoreType.DMA
    results = pl.pallas_call(
        functools.partial(ring_kernel, n, m),
        out_shape=tuple(pltpu.VMEM(*kind) for kind in kinds),
        in_specs=[hbm] * 12,
        out_specs=(vmem,) * 10,
        scratch_shapes=[
            pltpu.VMEM((2, tokens, width), bf16),
            pltpu.VMEM((2, tokens, columns), bf16),
            pltpu.VMEM((2, block, rank), bf16),
            pltpu.VMEM((2, block, columns), f32),
            pltpu.VMEM((2, low_rows, columns), f32),
            pltpu.VMEM((2, low_rows, columns), f32),
            pltpu.VMEM((2, part, block), bf16),
            pltpu.VMEM((2, n, part, block), bf16),
            pltpu.VMEM((2, m, 2, part, tokens), bf16),
            pltpu.VMEM((2, n, low_rows, columns), f32),
            pltpu.VMEM((2, n // 2, low_rows, columns), f32),
            pltpu.VMEM((2, n // 2, low_rows, columns), f32),
            pltpu.VMEM((n * m, 8, 128), f32),
            pltpu.VMEM((2, n, low_rows, columns), bf16),
            dma((6, 2)),
            dma((2, 2, n)),
            dma((2, 2, m)),
            dma((2, 2, n // 2)),
            dma((2, 2, n // 2)),
            dma((2, n * m)),
            dma((2, 2, n)),
            dma((2, 2, n - 1, CHUNKS)),
        ],
        compiler_params=pltpu.CompilerParams(
            collective_id=0, has_side_effects=True, vmem_limit_bytes=48 * 2**20
        ),
    )(*args)
    return pl.pallas_call(
        functools.partial(write_kernel, len(kinds)),
        out_shape=tuple(jax.ShapeDtypeStruct(*kind) for kind in kinds),
        in_specs=[pl.BlockSpec(memory_space=pl.ANY)] * len(kinds),
        out_specs=(hbm,) * len(kinds),
        scratch_shapes=[dma((len(kinds),))],
        compiler_params=pltpu.CompilerParams(vmem_limit_bytes=2**20),
    )(*results)


def fits(n, m, *args):
    basis, first = args[4], args[8]
    return (
        n % 2 == 0
        and basis.shape[1] // n % 16 == 0
        and basis.shape[1] // m % 16 == 0
        and basis.shape[0] // n % (16 * CHUNKS) == 0
        and basis.shape[0] // n % 128 == 0
        and first.shape[1] // m % 128 == 0
    )


def solution(mesh):
    placed = (
        P("fs", None),
        P("fs", "tp"),
        P("fs", None),
        P("fs", "tp"),
        P("fs", None),
        P("fs", None),
        P("fs", "tp"),
        P("fs", "tp"),
        P("fs", "tp"),
        P("fs", "tp"),
        P("fs", "tp"),
        P("fs", "tp"),
    )
    n, m = mesh.shape["fs"], mesh.shape["tp"]

    def step(*args):
        body = functools.partial(fused_per_device, n, m) if fits(n, m, *args) else per_device
        return jax.shard_map(
            body,
            mesh=mesh,
            in_specs=placed,
            out_specs=(P("fs", "tp"),) * 8 + (P(None, "tp"),) * 2,
            check_vma=False,
        )(*args)

    return step
```

time: 179 us -> 147 us (0.82)
  local copies, waits for them, and re-layouts: 19.3 us -> 0 us
  Pallas kernels: 159 us -> 146 us
    unnamed x34 -> x0, local copies, waits for them, and re-layouts: 19.3 us -> none
    pallas_call x1 -> x2, Pallas kernels: 159 us -> 146 us  [the longest x1 141 us: fused_per_device(): pl.pallas_call(functools.partial(ring_kernel, n, m), out_shape=tuple((plt...]
where the time goes in v2:
time: 147 us; the launch traced here: 146 us
  Pallas kernels  146 us (99%)
    pallas_call x1, Pallas kernels, fused_per_device(): pl.pallas_call(functools.partial(ring_kernel, n, m), out_shape=tuple((plt...  141 us
    pallas_call x1, Pallas kernels, fused_per_device(): pl.pallas_call(functools.partial(write_kernel, len(kinds)), out_shape=tup...  4.83 us

profile of v2, /device:TPU:0, one launch (start us, length us, event | category | flops | bytes accessed | tf_op | source)
XLA Modules:
  0.0 146.5 jit_solution(2350308580199239041)
XLA Ops:
  0.6 141.0 %shard_map.195 = (f32[512,512]{1,0:T(8,128)S(1)}, f32[512,512]{1,0:T(8,128)S(1)}, f32[512,512]{1,0:T(8,128)S(1)}, f32[512,512]{1,0:T(8,128)S(1)}, f32[32,512]{1,...) custom-call(bf16[256,4096]{1,0:T(8,128)(2,1)} %refs_0_.1, ...), custom_call_target="tpu_custom_call" | custom-call | tf_op jit(solution)/shard_map/pallas_call | solution.py:356
  141.7 4.8 %shard_map.196 = (f32[512,512]{1,0:T(8,128)}, f32[512,512]{1,0:T(8,128)}, f32[512,512]{1,0:T(8,128)}, f32[512,512]{1,0:T(8,128)}, f32[32,512]{1,0:T(8,128)}, /*i...) custom-call(f32[512,512]{1,0:T(8,128)S(1)} %get-tuple-element.20.ref, ...), custom_call_target="tpu_custom_call" | custom-call | tf_op jit(solution)/shard_map/pallas_call | solution.py:389

commit v3 on v2

--- a/solution.py
+++ b/solution.py
@@ -116,12 +116,13 @@
     )
     (
         x_v, cot_v, basis, master_v, first, second,
-        mine_v, rows_v, coord_v, part_v, pair_v, got_v, square_v, direction_v,
-        in_sem, rows_sem, coord_sem, pair_sem, part_sem, square_sem, direction_sem, gather_sem,
+        rows_v, ahead_v, wide_v, coord_v, part_v, pair_v, got_v, square_v, direction_v,
+        in_sem, rows_sem, coord_sem, pair_sem, part_sem, square_sem, direction_sem, gather_sem, ahead_sem, wide_sem,
     ) = refs[22:]
     f, t = lax.axis_index("fs"), lax.axis_index("tp")
     me = f * m + t
-    rank_part, block = mine_v.shape[1:]
+    rank_part, block = rows_v.shape[2:]
+    piece = block // CHUNKS
     rank = basis.shape[2]
     tokens = x_v.shape[1]
     columns = cot_v.shape[2]
@@ -162,7 +163,7 @@
     select = jnp.where(chosen, 1.0, 0.0).astype(jnp.bfloat16)
     for k in range(2):
         loads["basis", k].wait()
-        mine_v[k] = lax.dot_general(
+        rows_v[k, 0] = lax.dot_general(
             select, basis[k], (((1,), (1,)), ((), ())), preferred_element_type=jnp.float32
         ).astype(jnp.bfloat16)
     pl.semaphore_wait(barrier, n * m - 1)
@@ -196,15 +197,18 @@
     def rows_at(k):
         return lambda d: rows_v.at[k, d]
 
-    rows = [push(mine_v.at[k], rows_at(k), rows_sem, k) for k in range(2)]
+    rows = [push(rows_v.at[k, 0], rows_at(k), rows_sem, k) for k in range(2)]
 
     def coordinates(k, d):
         source = along(-(d % half), x if d < half else 1 - x)
-        left = mine_v[k] if d == 0 else rows_v[k, d]
+        left = rows_v[k, d]
         right = x_v[k, :, pl.ds(pl.multiple_of(source * block, block), block)]
         return lax.dot_general(left, right, (((1,), (1,)), ((), ())), preferred_element_type=jnp.float32)
 
-    coords = []
+    def ahead_at(k):
+        return lambda d: ahead_v.at[k, d]
+
+    coords, ahead = [], []
     for k in range(2):
         if k == 0:
             relay(rows[0], rows_at(0), rows_sem, 0)
@@ -214,6 +218,10 @@
             total = total + coordinates(k, d)
         if k == 0:
             relay(rows[1], rows_at(1), rows_sem, 1)
+            for i in range(2):
+                loads["master", i].wait()
+                ahead_v[i, 0] = master_v[i, pl.ds(0, piece)].astype(jnp.bfloat16)
+                ahead.append(push(ahead_v.at[i, 0], ahead_at(i), ahead_sem, i))
         for d in range(half, n):
             rows[k][d].wait_recv()
             total = total + coordinates(k, d)
@@ -227,6 +235,12 @@
             ]
         )
 
+    wide = []
+    for k in range(2):
+        source = rows_v.at[k, :, :, pl.ds(0, piece)]
+        for d in range(1, m):
+            wide.append(send(source, wide_v.at[k, t], wide_sem, (k, d), {"tp": lax.rem(t + d, m)}))
+        wide_v[k, t] = rows_v[k, :, :, :piece]
     pairs = []
     for k in range(2):
         loads["cot", k].wait()
@@ -243,6 +257,7 @@
             )
     parts = []
     for k in range(2):
+        relay(ahead[k], ahead_at(k), ahead_sem, k)
         parts.append({})
         for d in (1, half - 1, *range(2, half - 1)):
             pairs[k][d].wait_recv()
@@ -297,9 +312,7 @@
 
     toward = (at(place + 1), at(place - 1))
     origin = [[at(place - s), at(place + s)] for s in range(n)]
-    piece = block // CHUNKS
-    for k in range(2):
-        loads["master", k].wait()
+    for k in range(2):
         for d in range(half, n):
             directions[k][d].wait_recv()
     ring = {}
@@ -308,7 +321,7 @@
         where = gathered[k].at[pl.ds(pl.multiple_of(origin[s][k] * block + c * piece, piece), piece)]
         ring[s, k, c] = send(where, where, gather_sem, (k, s, c), {"fs": toward[k]})
 
-    for c in range(CHUNKS):
+    def own_piece(c):
         for k in range(2):
             span = pl.ds(c * piece, piece)
             step = jnp.dot(
@@ -317,16 +330,38 @@
                 preferred_element_type=jnp.float32,
             )
             weight = master_v[k, span, :] - rate * step
-            gathered[k][pl.ds(pl.multiple_of(f * block + c * piece, piece), piece)] = weight.astype(jnp.bfloat16)
-            forward(0, k, c)
+            if c > 0:
+                gathered[k][pl.ds(pl.multiple_of(f * block + c * piece, piece), piece)] = weight.astype(jnp.bfloat16)
+                forward(0, k, c)
             step_out[k][span] = step
             w_out[k][span] = weight
+    def finish_ahead(d):
+        source = along(-(d % half), x if d < half else 1 - x)
+        for k in range(2):
+            step = lax.dot_general(
+                wide_v[k, :, d].reshape(rank, piece),
+                direction_v[k].reshape(rank, columns),
+                (((0,), (0,)), ((), ())),
+                preferred_element_type=jnp.float32,
+            )
+            weight = ahead_v[k, d].astype(jnp.float32) - rate * step
+            gathered[k][pl.ds(pl.multiple_of(source * block, block), piece)] = weight.astype(jnp.bfloat16)
+
+    for c in (*range(1, CHUNKS), 0):
+        own_piece(c)
+    for copy in wide:
+        copy.wait_recv()
+    for k in range(2):
+        for d in range(half, n):
+            ahead[k][d].wait_recv()
+    finish_ahead(0)
     for s in range(1, n):
-        for c in range(CHUNKS):
+        for c in range(1, CHUNKS):
             for k in range(2):
                 ring[s - 1, k, c].wait_recv()
                 if s < n - 1:
                     forward(s, k, c)
+        finish_ahead(s)
     for copy in sent:
         copy.wait_send()
 
@@ -365,8 +400,9 @@
             pltpu.VMEM((2, block, columns), f32),
             pltpu.VMEM((2, low_rows, columns), f32),
             pltpu.VMEM((2, low_rows, columns), f32),
-            pltpu.VMEM((2, part, block), bf16),
             pltpu.VMEM((2, n, part, block), bf16),
+            pltpu.VMEM((2, n, block // CHUNKS, columns), bf16),
+            pltpu.VMEM((2, m, n, part, block // CHUNKS), bf16),
             pltpu.VMEM((2, m, 2, part, tokens), bf16),
             pltpu.VMEM((2, n, low_rows, columns), f32),
             pltpu.VMEM((2, n // 2, low_rows, columns), f32),
@@ -381,6 +417,8 @@
             dma((2, n * m)),
             dma((2, 2, n)),
             dma((2, 2, n - 1, CHUNKS)),
+            dma((2, 2, n)),
+            dma((2, 2, m)),
         ],
         compiler_params=pltpu.CompilerParams(
             collective_id=0, has_side_effects=True, vmem_limit_bytes=48 * 2**20
@@ -402,7 +440,7 @@
         n % 2 == 0
         and basis.shape[1] // n % 16 == 0
         and basis.shape[1] // m % 16 == 0
-        and basis.shape[0] // n % (16 * CHUNKS) == 0
+        and basis.shape[0] // n % (128 * CHUNKS) == 0
         and basis.shape[0] // n % 128 == 0
         and first.shape[1] // m % 128 == 0
     )

time: 147 us -> 139 us (0.946)
  Pallas kernels: 146 us -> 138 us
    pallas_call x1, Pallas kernels: 141 us -> 133 us  [fused_per_device(): pl.pallas_call(functools.partial(ring_kernel, n, m), out_shape=tuple((plt...]
where the time goes in v3:
time: 139 us
  Pallas kernels  138 us (99%)
    pallas_call x1, Pallas kernels, fused_per_device(): pl.pallas_call(functools.partial(ring_kernel, n, m), out_shape=tuple((plt...  133 us
    pallas_call x1, Pallas kernels, fused_per_device(): pl.pallas_call(functools.partial(write_kernel, len(kinds)), out_shape=tup...  4.83 us

profile of v3, /device:TPU:0, one launch (start us, length us, event | category | flops | bytes accessed | tf_op | source)
XLA Modules:
  0.0 138.9 jit_solution(9051862319218272233)
XLA Ops:
  0.6 133.4 %shard_map.195 = (f32[512,512]{1,0:T(8,128)S(1)}, f32[512,512]{1,0:T(8,128)S(1)}, f32[512,512]{1,0:T(8,128)S(1)}, f32[512,512]{1,0:T(8,128)S(1)}, f32[32,512]{1,...) custom-call(bf16[256,4096]{1,0:T(8,128)(2,1)} %refs_0_.1, ...), custom_call_target="tpu_custom_call" | custom-call | tf_op jit(solution)/shard_map/pallas_call | solution.py:391
  134.1 4.8 %shard_map.196 = (f32[512,512]{1,0:T(8,128)}, f32[512,512]{1,0:T(8,128)}, f32[512,512]{1,0:T(8,128)}, f32[512,512]{1,0:T(8,128)}, f32[32,512]{1,0:T(8,128)}, /*i...) custom-call(f32[512,512]{1,0:T(8,128)S(1)} %get-tuple-element.20.ref, ...), custom_call_target="tpu_custom_call" | custom-call | tf_op jit(solution)/shard_map/pallas_call | solution.py:427

commit v4 on v3

--- a/solution.py
+++ b/solution.py
@@ -116,7 +116,7 @@
     )
     (
         x_v, cot_v, basis, master_v, first, second,
-        rows_v, ahead_v, wide_v, coord_v, part_v, pair_v, got_v, square_v, direction_v,
+        rows_v, ahead_v, wide_v, flat_v, coord_v, part_v, pair_v, got_v, square_v, direction_v,
         in_sem, rows_sem, coord_sem, pair_sem, part_sem, square_sem, direction_sem, gather_sem, ahead_sem, wide_sem,
     ) = refs[22:]
     f, t = lax.axis_index("fs"), lax.axis_index("tp")
@@ -281,6 +281,11 @@
         copies.append(
             send(square_v.at[0], square_v.at[d], square_sem, (d,), {"fs": other // m, "tp": lax.rem(other, m)})
         )
+    for copy in wide:
+        copy.wait_recv()
+    for k in range(2):
+        for d in range(n):
+            flat_v[k, d] = wide_v[k, :, d].reshape(rank, piece).T
     for k in range(2):
         loads["first", k].wait()
         loads["second", k].wait()
@@ -335,33 +340,29 @@
                 forward(0, k, c)
             step_out[k][span] = step
             w_out[k][span] = weight
-    def finish_ahead(d):
+    def finish_ahead(k, d):
         source = along(-(d % half), x if d < half else 1 - x)
-        for k in range(2):
-            step = lax.dot_general(
-                wide_v[k, :, d].reshape(rank, piece),
-                direction_v[k].reshape(rank, columns),
-                (((0,), (0,)), ((), ())),
-                preferred_element_type=jnp.float32,
-            )
-            weight = ahead_v[k, d].astype(jnp.float32) - rate * step
-            gathered[k][pl.ds(pl.multiple_of(source * block, block), piece)] = weight.astype(jnp.bfloat16)
+        if d >= half:
+            ahead[k][d].wait_recv()
+        step = jnp.dot(
+            flat_v[k, d], direction_v[k].reshape(rank, columns), preferred_element_type=jnp.float32
+        )
+        weight = ahead_v[k, d].astype(jnp.float32) - rate * step
+        gathered[k][pl.ds(pl.multiple_of(source * block, block), piece)] = weight.astype(jnp.bfloat16)
 
     for c in (*range(1, CHUNKS), 0):
         own_piece(c)
-    for copy in wide:
-        copy.wait_recv()
-    for k in range(2):
-        for d in range(half, n):
-            ahead[k][d].wait_recv()
-    finish_ahead(0)
+    units = [(k, d) for d in range(n) for k in range(2)]
     for s in range(1, n):
         for c in range(1, CHUNKS):
             for k in range(2):
                 ring[s - 1, k, c].wait_recv()
                 if s < n - 1:
                     forward(s, k, c)
-        finish_ahead(s)
+            if units:
+                finish_ahead(*units.pop(0))
+    for unit in units:
+        finish_ahead(*unit)
     for copy in sent:
         copy.wait_send()
 
@@ -403,6 +404,7 @@
             pltpu.VMEM((2, n, part, block), bf16),
             pltpu.VMEM((2, n, block // CHUNKS, columns), bf16),
             pltpu.VMEM((2, m, n, part, block // CHUNKS), bf16),
+            pltpu.VMEM((2, n, block // CHUNKS, rank), bf16),
             pltpu.VMEM((2, m, 2, part, tokens), bf16),
             pltpu.VMEM((2, n, low_rows, columns), f32),
             pltpu.VMEM((2, n // 2, low_rows, columns), f32),

time: 139 us -> 139 us (level)
  no operation moved by 1% of the time
where the time goes in v4:
time: 139 us
  Pallas kernels  138 us (99%)
    pallas_call x1, Pallas kernels, fused_per_device(): pl.pallas_call(functools.partial(ring_kernel, n, m), out_shape=tuple((plt...  133 us
    pallas_call x1, Pallas kernels, fused_per_device(): pl.pallas_call(functools.partial(write_kernel, len(kinds)), out_shape=tup...  4.83 us

profile of v4, /device:TPU:0, one launch (start us, length us, event | category | flops | bytes accessed | tf_op | source)
XLA Modules:
  0.0 138.7 jit_solution(6494381888606846717)
XLA Ops:
  0.6 133.2 %shard_map.195 = (f32[512,512]{1,0:T(8,128)S(1)}, f32[512,512]{1,0:T(8,128)S(1)}, f32[512,512]{1,0:T(8,128)S(1)}, f32[512,512]{1,0:T(8,128)S(1)}, f32[32,512]{1,...) custom-call(bf16[256,4096]{1,0:T(8,128)(2,1)} %refs_0_.1, ...), custom_call_target="tpu_custom_call" | custom-call | tf_op jit(solution)/shard_map/pallas_call | solution.py:392
  133.8 4.8 %shard_map.196 = (f32[512,512]{1,0:T(8,128)}, f32[512,512]{1,0:T(8,128)}, f32[512,512]{1,0:T(8,128)}, f32[512,512]{1,0:T(8,128)}, f32[32,512]{1,0:T(8,128)}, /*i...) custom-call(f32[512,512]{1,0:T(8,128)S(1)} %get-tuple-element.20.ref, ...), custom_call_target="tpu_custom_call" | custom-call | tf_op jit(solution)/shard_map/pallas_call | solution.py:429

commit v5 on v4

--- a/solution.py
+++ b/solution.py
@@ -257,12 +257,12 @@
             )
     parts = []
     for k in range(2):
-        relay(ahead[k], ahead_at(k), ahead_sem, k)
         parts.append({})
         for d in (1, half - 1, *range(2, half - 1)):
             pairs[k][d].wait_recv()
             pair_v[k, d] = pair_v[k, d] + part_v[k, along(d)]
             parts[k][d] = send(pair_v.at[k, d], got_v.at[k, d], part_sem, (k, d), {"fs": along(d)})
+        relay(ahead[k], ahead_at(k), ahead_sem, k)
 
     lows = []
     squares = jnp.zeros((), jnp.float32)

time: 139 us -> 138 us (level)
  no operation moved by 1% of the time
where the time goes in v5:
time: 138 us
  Pallas kernels  138 us (100%)
    pallas_call x1, Pallas kernels, fused_per_device(): pl.pallas_call(functools.partial(ring_kernel, n, m), out_shape=tuple((plt...  133 us
    pallas_call x1, Pallas kernels, fused_per_device(): pl.pallas_call(functools.partial(write_kernel, len(kinds)), out_shape=tup...  4.83 us

profile of v5, /device:TPU:0, one launch (start us, length us, event | category | flops | bytes accessed | tf_op | source)
XLA Modules:
  0.0 138.2 jit_solution(8725757504756499722)
XLA Ops:
  0.6 132.7 %shard_map.195 = (f32[512,512]{1,0:T(8,128)S(1)}, f32[512,512]{1,0:T(8,128)S(1)}, f32[512,512]{1,0:T(8,128)S(1)}, f32[512,512]{1,0:T(8,128)S(1)}, f32[32,512]{1,...) custom-call(bf16[256,4096]{1,0:T(8,128)(2,1)} %refs_0_.1, ...), custom_call_target="tpu_custom_call" | custom-call | tf_op jit(solution)/shard_map/pallas_call | solution.py:392
  133.4 4.8 %shard_map.196 = (f32[512,512]{1,0:T(8,128)}, f32[512,512]{1,0:T(8,128)}, f32[512,512]{1,0:T(8,128)}, f32[512,512]{1,0:T(8,128)}, f32[32,512]{1,0:T(8,128)}, /*i...) custom-call(f32[512,512]{1,0:T(8,128)S(1)} %get-tuple-element.20.ref, ...), custom_call_target="tpu_custom_call" | custom-call | tf_op jit(solution)/shard_map/pallas_call | solution.py:429
